TPU v7x, 32 devices: a whole 2x2x4 slice. The times are simulated.
32 devices in a mesh: grp: 2 (over y), sp: 4 (over z), dp: 4 (over x, core).
Axes of the slice: x: 2, y: 2, z: 4, core: 2. Of those that a mesh axis runs over, the one named last changes fastest.
Arguments:
- query_rows: bfloat16 [8, 512, 2048], P(('grp', 'dp'), 'sp'), parts along dimension 0, may hold values from -6 to 6
- key_rows: bfloat16 [8, 512, 2048], P(('grp', 'dp'), 'sp'), parts along dimension 0, may hold values from -6 to 6
- value_rows: bfloat16 [8, 512, 2048], P(('grp', 'dp'), 'sp'), parts along dimension 0, may hold values from -6 to 6
- query_gain: float32 [64], replicated, may hold values from 1.1 to 7
- key_gain: float32 [64], replicated, may hold values from 1.1 to 7
- lambdas: float32 [16], replicated, may hold values from 0.3 to 0.8
- head_gain: float32 [128], replicated, may hold values from 0.1 to 1.9
- out_weight: bfloat16 [2048, 2048], P(None, 'dp'), may hold values from -0.125 to 0.125
Outputs:
- attended: bfloat16 [8, 512, 2048], P(('grp', 'dp'), 'sp'), parts along dimension 0
There are 2 independent parts, one for each index of `grp`. A program takes and returns all parts, laid end to end along the dimension named above; an argument that names none is the same for every part. Nothing has to cross between parts.
All inputs are finite; a program needn't handle non-finite values.
Results may differ from a plain program's by a relative error of at most 0.008.
The roundings to bfloat16 on the way count: a program that leaves them out, or rounds other values in their place, can miss the bound.
Values may be sent and summed in bfloat16 or wider, within the bound.
A program may use at most 128 MiB of HBM per device.

v0:
```python
import jax
import jax.numpy as jnp
from jax import lax
from jax.sharding import PartitionSpec as P

EPSILON = 1e-06
OUT_SCALE = 0.8


def norm_rotate(field_rows, gain_vector, positions):
    widened = field_rows.astype(jnp.float32)
    normed = (
        widened
        * lax.rsqrt(jnp.mean(widened * widened, axis=-1, keepdims=True) + EPSILON)
        * gain_vector
    )
    half_size = field_rows.shape[-1] // 2
    inverse = 10000.0 ** (-jnp.arange(half_size, dtype=jnp.float32) / half_size)
    angles = (positions[:, None] * inverse[None, :]).reshape(positions.shape[0], 1, 1, half_size)
    cosine_part = jnp.cos(angles)
    sine_part = jnp.sin(angles)
    first_half = normed[..., :half_size]
    second_half = normed[..., half_size:]
    turned = jnp.concatenate(
        [
            first_half * cosine_part - second_half * sine_part,
            second_half * cosine_part + first_half * sine_part,
        ],
        axis=-1,
    )
    return turned.astype(jnp.bfloat16)


def head_norm(raw_heads, gain_vector):
    scaled = raw_heads * lax.rsqrt(
        jnp.mean(raw_heads * raw_heads, axis=-1, keepdims=True) + EPSILON
    )
    return (scaled * gain_vector * OUT_SCALE).astype(jnp.bfloat16)


def block_size():
    return 512


def attend(query_head, key_head, value_head, weight_two, gain_vector):
    length = query_head.shape[0]
    block_rows = block_size()
    score_scale = query_head.shape[-1] ** (-0.5)
    offsets = jnp.arange(block_rows, dtype=jnp.int32)
    value_size = value_head.shape[-1]

    def one_block(number):
        first_row = number * block_rows
        query_block = lax.dynamic_slice_in_dim(query_head, first_row, block_rows, 0)
        query_positions = first_row + offsets

        def fill_scores(kblock, buffer):
            key_block = lax.dynamic_slice_in_dim(key_head, kblock * block_rows, block_rows, 0)
            scores = (
                jnp.einsum(
                    "qcd,kcd->cqk", query_block, key_block, preferred_element_type=jnp.float32
                )
                * score_scale
            )
            visible = (kblock * block_rows + offsets)[None, :] <= query_positions[:, None]
            scores = jnp.where(visible[None], scores, -1e30)
            return lax.dynamic_update_slice_in_dim(buffer, scores, kblock * block_rows, 2)

        start_buffer = jnp.full((2, block_rows, length), -1e30, jnp.float32)
        stored = lax.fori_loop(0, number + 1, fill_scores, start_buffer)
        highest = jnp.max(stored, axis=-1)
        totals = jnp.sum(jnp.exp(stored - highest[..., None]), axis=-1)

        def weigh_values(kblock, accumulated):
            scores = lax.dynamic_slice_in_dim(stored, kblock * block_rows, block_rows, 2)
            probabilities = jnp.exp(scores - highest[..., None]) / totals[..., None]
            mixing = (probabilities[0] - weight_two * probabilities[1]).astype(jnp.bfloat16)
            value_block = lax.dynamic_slice_in_dim(value_head, kblock * block_rows, block_rows, 0)
            return accumulated + jnp.dot(mixing, value_block, preferred_element_type=jnp.float32)

        return lax.fori_loop(
            0, number + 1, weigh_values, jnp.zeros((block_rows, value_size), jnp.float32)
        )

    blocks = lax.map(one_block, jnp.arange(length // block_rows, dtype=jnp.int32))
    return head_norm(blocks.reshape(length, value_size), gain_vector)


def local(query_rows, key_rows, value_rows, query_gain, key_gain, lambdas, head_gain, out_weight):
    tok_count = query_rows.shape[1]
    group_size = lax.axis_size("sp")
    head_size = query_gain.shape[0]
    value_size = head_gain.shape[0]
    heads_total = lambdas.shape[0]
    local_heads = heads_total // group_size

    def by_peer(tensor):
        return tensor.reshape(1, tok_count, group_size, tensor.shape[2] // group_size)

    query_in, key_in, value_in = (
        lax.all_to_all(by_peer(query_rows), "sp", split_axis=2, concat_axis=1, tiled=True),
        lax.all_to_all(by_peer(key_rows), "sp", split_axis=2, concat_axis=1, tiled=True),
        lax.all_to_all(by_peer(value_rows), "sp", split_axis=2, concat_axis=1, tiled=True),
    )
    length = tok_count * group_size
    positions = jnp.arange(length, dtype=jnp.float32)
    query_rot = norm_rotate(
        query_in.reshape(length, local_heads, 2, head_size), query_gain, positions
    )
    key_rot = norm_rotate(key_in.reshape(length, local_heads, 2, head_size), key_gain, positions)
    value_heads = value_in.reshape(length, local_heads, value_size)
    local_lambdas = lax.dynamic_slice_in_dim(
        lambdas, lax.axis_index("sp") * local_heads, local_heads
    )

    def per_head(head_index):
        return attend(
            query_rot[:, head_index],
            key_rot[:, head_index],
            value_heads[:, head_index],
            local_lambdas[head_index],
            head_gain,
        )

    outputs = lax.map(per_head, jnp.arange(local_heads, dtype=jnp.int32))
    outputs = jnp.transpose(outputs, (1, 0, 2)).reshape(1, length, 1, local_heads * value_size)
    returned = lax.all_to_all(outputs, "sp", split_axis=1, concat_axis=2, tiled=True)
    heads_rows = returned.reshape(tok_count, heads_total * value_size)
    attended = jnp.dot(
        heads_rows,
        lax.all_gather(out_weight, "dp", axis=1, tiled=True),
        preferred_element_type=jnp.float32,
    )
    return attended.astype(jnp.bfloat16).reshape(1, tok_count, attended.shape[1])


def solution(mesh):
    placed = (
        P(("grp", "dp"), "sp", None),
        P(("grp", "dp"), "sp", None),
        P(("grp", "dp"), "sp", None),
        P(),
        P(),
        P(),
        P(),
        P(None, "dp"),
    )
    return jax.shard_map(
        local, mesh=mesh, in_specs=placed, out_specs=P(("grp", "dp"), "sp", None), check_vma=False
    )
```

profile of v0, /device:TPU:0, one launch (start us, length us, event | category | flops | bytes accessed | tf_op | source)
XLA Modules:
  0.0 130.4 jit_solution(3775947803156317788)
XLA Ops:
  6.5 0.7 all-gather.2.cloned.1.call-update
  7.6 1.0 copy.25
  8.6 6.3 %all-to-all-start = ((bf16[1,128,4,512]{1,3,0,2:T(8,128)(2,1)}), bf16[1,128,4,512]{1,3,0,2:T(8,128)(2,1)S(1)}, u32[]{:S(2)}, u32[]{:S(2)}) async-start(bf16[1,128,4,512]{1,3,0,2:T(8,128)(2,1)} %bitcast.7), calls=%async_computation | async-start | bytes 1048576 | tf_op jit(solution)/shard_map/all_to_all | solution.py:102
  15.0 1.0 copy.27
  16.0 13.5 %all-to-all-done = bf16[1,128,4,512]{1,3,0,2:T(8,128)(2,1)S(1)} async-done(((bf16[1,128,4,512]{1,3,0,2:T(8,128)(2,1)}), bf16[1,128,4,512]{1,3,0,2:T(8,128)(2,1)S(1)}, u32[]{:S(2)}, u32[]{:S(2)}) %all-to-all-start) | async-done | bytes 524320 | tf_op jit(solution)/shard_map/all_to_all | solution.py:102
  29.5 3.6 %all-to-all-start.1 = ((bf16[1,128,4,512]{1,3,0,2:T(8,128)(2,1)}), bf16[1,128,4,512]{1,3,0,2:T(8,128)(2,1)S(1)}, u32[]{:S(2)}, u32[]{:S(2)}) async-start(bf16[1,128,4,512]{1,3,0,2:T(8,128)(2,1)} %bitcast.10), calls=%async_computation.1 | async-start | bytes 1048576 | tf_op jit(solution)/shard_map/all_to_all | solution.py:101
  33.4 1.1 copy.30
  34.4 12.7 %all-to-all-done.1 = bf16[1,128,4,512]{1,3,0,2:T(8,128)(2,1)S(1)} async-done(((bf16[1,128,4,512]{1,3,0,2:T(8,128)(2,1)}), bf16[1,128,4,512]{1,3,0,2:T(8,128)(2,1)S(1)}, u32[]{:S(2)}, u32[]{:S(2)}) %all-to-all-start.1) | async-done | bytes 524320 | tf_op jit(solution)/shard_map/all_to_all | solution.py:101
  47.1 4.1 %all-to-all-start.2 = ((bf16[1,128,4,512]{3,1,0,2:T(8,128)(2,1)}), bf16[1,128,4,512]{3,1,0,2:T(8,128)(2,1)}, u32[]{:S(2)}, u32[]{:S(2)}) async-start(bf16[1,128,4,512]{3,1,0,2:T(8,128)(2,1)} %copy.30), calls=%async_computation.2 | async-start | bytes 1048576 | tf_op jit(solution)/shard_map/all_to_all | solution.py:103
  51.7 0.7 copy.26
  52.9 0.7 copy.28
  54.0 11.3 %all-to-all-done.2 = bf16[1,128,4,512]{3,1,0,2:T(8,128)(2,1)} async-done(((bf16[1,128,4,512]{3,1,0,2:T(8,128)(2,1)}), bf16[1,128,4,512]{3,1,0,2:T(8,128)(2,1)}, u32[]{:S(2)}, u32[]{:S(2)}) %all-to-all-start.2) | async-done | bytes 524320 | tf_op jit(solution)/shard_map/all_to_all | solution.py:103
  65.3 1.2 reshape.147
  67.9 1.1 pad_maximum_fusion
  69.0 26.1 %while.54 = (s32[]{:T(128)}, bf16[4,512,128]{1,2,0:T(8,128)(2,1)S(1)}, s32[4]{0:T(128)S(1)}, bf16[512,4,2,64]{0,3,2,1:T(8,128)(2,1)}, bf16[512,4,2,64]{0,3,2,1:T...) while((s32[]{:T(128)}, ...), condition=%wide.region_8.9_spmd, body=%wide.region_2.8_spmd.sunk | while | flops 138281984 | bytes 9979571 | solution.py:125
  69.0 0.6 dynamic_slice.79
  71.6 2.0 %fusion.54 = (f32[2,512]{1,0:T(2,128)S(1)}, f32[2,512,512]{1,2,0:T(8,128)S(1)}) fusion(pred[512,512]{0,1:T(8,128)(4,1)S(1)} %iota_compare_fusion.2, bf16[512,4,2,64]{0,3,2,1:T(8,128)(2,1)} %get-tuple-element.419, s32[]{:T(128)S(6)} %select_n.36, bf16[512,4,2,64]{0,3,2,1:T(8,128)(2,1)} %get-tuple-element.420), kind=kOutput, calls=%fused_computation.57.clone.1 | convolution fusion | flops 69206528 | bytes 2626560 | tf_op jit(solution)/shard_map/while/body/eval_jaxpr/while/body/eval_jaxpr/sub | solution.py:72
  73.9 0.6 dynamic_slice.80
  74.4 0.9 multiply_reduce_fusion.4
  78.1 2.0 %fusion.54 = (f32[2,512]{1,0:T(2,128)S(1)}, f32[2,512,512]{1,2,0:T(8,128)S(1)}) fusion(pred[512,512]{0,1:T(8,128)(4,1)S(1)} %iota_compare_fusion.2, bf16[512,4,2,64]{0,3,2,1:T(8,128)(2,1)} %get-tuple-element.419, s32[]{:T(128)S(6)} %select_n.36, bf16[512,4,2,64]{0,3,2,1:T(8,128)(2,1)} %get-tuple-element.420), kind=kOutput, calls=%fused_computation.57.clone.1 | convolution fusion | flops 69206528 | bytes 2626560 | tf_op jit(solution)/shard_map/while/body/eval_jaxpr/while/body/eval_jaxpr/sub | solution.py:72
  80.4 0.6 dynamic_slice.80
  81.0 0.9 multiply_reduce_fusion.4
  84.7 2.0 %fusion.54 = (f32[2,512]{1,0:T(2,128)S(1)}, f32[2,512,512]{1,2,0:T(8,128)S(1)}) fusion(pred[512,512]{0,1:T(8,128)(4,1)S(1)} %iota_compare_fusion.2, bf16[512,4,2,64]{0,3,2,1:T(8,128)(2,1)} %get-tuple-element.419, s32[]{:T(128)S(6)} %select_n.36, bf16[512,4,2,64]{0,3,2,1:T(8,128)(2,1)} %get-tuple-element.420), kind=kOutput, calls=%fused_computation.57.clone.1 | convolution fusion | flops 69206528 | bytes 2626560 | tf_op jit(solution)/shard_map/while/body/eval_jaxpr/while/body/eval_jaxpr/sub | solution.py:72
  86.9 0.6 dynamic_slice.80
  87.5 0.9 multiply_reduce_fusion.4
  91.2 2.0 %fusion.54 = (f32[2,512]{1,0:T(2,128)S(1)}, f32[2,512,512]{1,2,0:T(8,128)S(1)}) fusion(pred[512,512]{0,1:T(8,128)(4,1)S(1)} %iota_compare_fusion.2, bf16[512,4,2,64]{0,3,2,1:T(8,128)(2,1)} %get-tuple-element.419, s32[]{:T(128)S(6)} %select_n.36, bf16[512,4,2,64]{0,3,2,1:T(8,128)(2,1)} %get-tuple-element.420), kind=kOutput, calls=%fused_computation.57.clone.1 | convolution fusion | flops 69206528 | bytes 2626560 | tf_op jit(solution)/shard_map/while/body/eval_jaxpr/while/body/eval_jaxpr/sub | solution.py:72
  93.4 0.6 dynamic_slice.80
  94.0 0.9 multiply_reduce_fusion.4
  95.1 0.9 copy.32
  96.5 3.8 %reduce = bf16[512,512]{1,0:T(8,128)(2,1)S(1)} reduce(bf16[512,1,1,512]{3,2,1,0:T(2,128)(2,1)S(1)} %bitcast.87, bf16[]{:T(256)} %broadcast.175), dimensions={1,2}, to_apply=%bitcast.59.reduce_sub_computation | reduce | bytes 1048578
  100.7 16.4 %all_to_all.48 = bf16[4,2,32768]{2,1,0:T(2,128)(2,1)S(1)} all-to-all(bf16[4,2,32768]{2,1,0:T(2,128)(2,1)S(1)} %reshape.155), channel_id=1, replica_groups=mesh['grp'=2,'sp'=4,'dp'=4] {'sp'}, dimensions={0} | all-to-all | bytes 1048576 | tf_op jit(solution)/shard_map/all_to_all | solution.py:127
  118.1 5.5 %fusion.38 = bf16[1,128,2048]{2,1,0:T(8,128)(2,1)} fusion(bf16[128,2048]{0,1:T(8,128)(2,1)S(1)} %bitcast.85, bf16[2048,2048]{1,0:T(8,128)(2,1)} %all-gather.2.cloned.1.call-done), kind=kOutput, calls=%fused_computation.38 | convolution fusion | flops 1074003968 | bytes 9437184 | tf_op jit(solution)/shard_map/dot_general | solution.py:129
  (60 shorter events, 8.7 us)
Async XLA Ops:
  6.5 1.0 copy-start.1
  6.5 8.4 %copy-start.2 = (bf16[1,128,2048]{2,1,0:T(8,128)(2,1)S(1)}, bf16[1,128,2048]{2,1,0:T(8,128)(2,1)}, u32[]{:S(2)}) copy-start(bf16[1,128,2048]{2,1,0:T(8,128)(2,1)} %param.12) | copy-start | bytes 1572868
  6.5 111.5 %all-gather.2.cloned.1.call-start = ((), (), s32[]{:S(2)}) async-start(), calls=%async_computation.4 | async-start | bytes 10485760 | tf_op jit(solution)/shard_map/all_gather | solution.py:131
  7.6 25.5 %copy-start.3 = (bf16[1,128,2048]{2,1,0:T(8,128)(2,1)S(1)}, bf16[1,128,2048]{2,1,0:T(8,128)(2,1)}, u32[]{:S(2)}) copy-start(bf16[1,128,2048]{2,1,0:T(8,128)(2,1)} %param.14) | copy-start | bytes 1572868
  8.6 20.8 %all-to-all-start = ((bf16[1,128,4,512]{1,3,0,2:T(8,128)(2,1)}), bf16[1,128,4,512]{1,3,0,2:T(8,128)(2,1)S(1)}, u32[]{:S(2)}, u32[]{:S(2)}) async-start(bf16[1,128,4,512]{1,3,0,2:T(8,128)(2,1)} %bitcast.7), calls=%async_computation | async-start | bytes 1048576 | tf_op jit(solution)/shard_map/all_to_all | solution.py:102
  29.5 21.8 %copy-start.7 = (f32[16]{0:T(128)S(1)}, f32[16]{0:T(128)}, u32[]{:S(2)}) copy-start(f32[16]{0:T(128)} %param.17) | copy-start | bytes 196
  29.5 17.6 %all-to-all-start.1 = ((bf16[1,128,4,512]{1,3,0,2:T(8,128)(2,1)}), bf16[1,128,4,512]{1,3,0,2:T(8,128)(2,1)S(1)}, u32[]{:S(2)}, u32[]{:S(2)}) async-start(bf16[1,128,4,512]{1,3,0,2:T(8,128)(2,1)} %bitcast.10), calls=%async_computation.1 | async-start | bytes 1048576 | tf_op jit(solution)/shard_map/all_to_all | solution.py:101
  47.1 18.2 %all-to-all-start.2 = ((bf16[1,128,4,512]{3,1,0,2:T(8,128)(2,1)}), bf16[1,128,4,512]{3,1,0,2:T(8,128)(2,1)}, u32[]{:S(2)}, u32[]{:S(2)}) async-start(bf16[1,128,4,512]{3,1,0,2:T(8,128)(2,1)} %copy.30), calls=%async_computation.2 | async-start | bytes 1048576 | tf_op jit(solution)/shard_map/all_to_all | solution.py:103
  65.3 1.6 %copy-start.5 = (f32[64]{0:T(128)S(1)}, f32[64]{0:T(128)}, u32[]{:S(2)}) copy-start(f32[64]{0:T(128)} %param.16) | copy-start | bytes 772
  66.6 0.7 copy-start.6
  67.5 1.5 %copy-start = (bf16[4,512,128]{1,2,0:T(8,128)(2,1)S(1)}, bf16[4,512,128]{1,2,0:T(8,128)(2,1)}, u32[]{:S(2)}) copy-start(bf16[4,512,128]{1,2,0:T(8,128)(2,1)} %custom-call) | copy-start | bytes 1572868
  67.5 1.5 %copy-start.4 = (f32[128]{0:T(128)S(1)}, f32[128]{0:T(128)}, u32[]{:S(2)}) copy-start(f32[128]{0:T(128)} %param.18) | copy-start | bytes 1540
Sparse Core Ops, SparseCore 0:
  8.9 60.9 all-gather.1
where the time goes:
time: 131 us; the launch traced here: 130 us
  waiting for transfers between devices  38.2 us (29%)
  matrix products  17.1 us (13%)
  blocking collectives  16.4 us (13%)
  local copies, waits for them, and re-layouts  14.6 us (11%)
  starting transfers between devices  14.1 us (11%)
  between operations  13.6 us (10%)
  other arithmetic  8.36 us (6%)
  loops' own time  7.96 us (6%)
    all_to_all x1, blocking collectives, local(): lax.all_to_all(outputs, 'sp', split_axis=1, concat_axis=2, tiled=True)  16.4 us
    all_to_all x1, waiting for transfers between devices, local(): lax.all_to_all(by_peer(key_rows), 'sp', split_axis=2, concat_axis=1, tile...  13.5 us
    all_to_all x1, waiting for transfers between devices, local(): lax.all_to_all(by_peer(query_rows), 'sp', split_axis=2, concat_axis=1, ti...  12.7 us
    all_to_all x1, waiting for transfers between devices, local(): lax.all_to_all(by_peer(value_rows), 'sp', split_axis=2, concat_axis=1, ti...  11.3 us
    another operation x1, loops' own time, local(): outputs = lax.map(per_head, jnp.arange(local_heads, dtype=jnp.int32))  7.96 us
    sub x4, matrix products, one_block(): totals = jnp.sum(jnp.exp(stored - highest[..., None]), axis=-1)  7.85 us
    all_to_all x1, starting transfers between devices, local(): lax.all_to_all(by_peer(key_rows), 'sp', split_axis=2, concat_axis=1, tile...  6.35 us
    dot_general x1, matrix products, local(): jnp.dot(heads_rows, lax.all_gather(out_weight, 'dp', axis=1, tiled=True),...  5.46 us
  transfers between devices with their start and end apart: 4, of which 3 were waited for; matrix products, arithmetic and copies ran while one was open for 26% of the time, Pallas kernels for 0%

commit v1 on v0

--- a/solution.py
+++ b/solution.py
@@ -5,6 +5,9 @@
 
 EPSILON = 1e-06
 OUT_SCALE = 0.8
+view_layers_all = lambda z_in: jnp.concatenate(
+    lax.all_to_all(jnp.stack(jnp.split(z_in, lax.axis_size("sp"), 1)), "sp", 0, 0), 2
+)
 
 
 def norm_rotate(field_rows, gain_vector, positions):
@@ -124,7 +127,7 @@
 
     outputs = lax.map(per_head, jnp.arange(local_heads, dtype=jnp.int32))
     outputs = jnp.transpose(outputs, (1, 0, 2)).reshape(1, length, 1, local_heads * value_size)
-    returned = lax.all_to_all(outputs, "sp", split_axis=1, concat_axis=2, tiled=True)
+    returned = view_layers_all(outputs)
     heads_rows = returned.reshape(tok_count, heads_total * value_size)
     attended = jnp.dot(
         heads_rows,

time: 131 us -> 125 us (0.954)
  other arithmetic: 8.36 us -> 4.63 us
  local copies, waits for them, and re-layouts: 14.6 us -> 12.1 us
    unnamed x1 -> x0, other arithmetic: 3.82 us -> none
    unnamed x23 -> x19, local copies, waits for them, and re-layouts: 4.21 us -> 2.69 us
  transfers between devices with their start and end apart: 4 -> 4, of which waited for: 3 -> 3; matrix products, arithmetic and copies ran while one was open for 26% -> 23% of each run, Pallas kernels for 0% -> 0%
where the time goes in v1:
time: 125 us; the launch traced here: 124 us
  waiting for transfers between devices  38.2 us (31%)
  matrix products  17.1 us (14%)
  blocking collectives  16.4 us (13%)
  starting transfers between devices  14.1 us (11%)
  between operations  13.6 us (11%)
  local copies, waits for them, and re-layouts  12.1 us (10%)
  loops' own time  7.96 us (6%)
  other arithmetic  4.63 us (4%)
    all_to_all x1, blocking collectives, lax.all_to_all(jnp.stack(jnp.split(z_in, lax.axis_size('sp'), 1)), 'sp',...  16.4 us
    all_to_all x1, waiting for transfers between devices, local(): lax.all_to_all(by_peer(key_rows), 'sp', split_axis=2, concat_axis=1, tile...  13.5 us
    all_to_all x1, waiting for transfers between devices, local(): lax.all_to_all(by_peer(query_rows), 'sp', split_axis=2, concat_axis=1, ti...  12.7 us
    all_to_all x1, waiting for transfers between devices, local(): lax.all_to_all(by_peer(value_rows), 'sp', split_axis=2, concat_axis=1, ti...  11.3 us
    another operation x1, loops' own time, local(): outputs = lax.map(per_head, jnp.arange(local_heads, dtype=jnp.int32))  7.96 us
    sub x4, matrix products, one_block(): totals = jnp.sum(jnp.exp(stored - highest[..., None]), axis=-1)  7.85 us
    all_to_all x1, starting transfers between devices, local(): lax.all_to_all(by_peer(key_rows), 'sp', split_axis=2, concat_axis=1, tile...  6.35 us
    dot_general x1, matrix products, local(): jnp.dot(heads_rows, lax.all_gather(out_weight, 'dp', axis=1, tiled=True),...  5.46 us
  transfers between devices with their start and end apart: 4, of which 3 were waited for; matrix products, arithmetic and copies ran while one was open for 23% of the time, Pallas kernels for 0%

profile of v1, /device:TPU:0, one launch (start us, length us, event | category | flops | bytes accessed | tf_op | source)
XLA Modules:
  0.0 124.0 jit_solution(939778945097915328)
XLA Ops:
  6.5 0.7 all-gather.2.cloned.1.call-update
  7.6 1.0 copy.21
  8.6 6.3 %all-to-all-start = ((bf16[1,128,4,512]{1,3,0,2:T(8,128)(2,1)}), bf16[1,128,4,512]{1,3,0,2:T(8,128)(2,1)S(1)}, u32[]{:S(2)}, u32[]{:S(2)}) async-start(bf16[1,128,4,512]{1,3,0,2:T(8,128)(2,1)} %bitcast.7), calls=%async_computation | async-start | bytes 1048576 | tf_op jit(solution)/shard_map/all_to_all | solution.py:105
  15.0 1.0 copy.23
  16.0 13.5 %all-to-all-done = bf16[1,128,4,512]{1,3,0,2:T(8,128)(2,1)S(1)} async-done(((bf16[1,128,4,512]{1,3,0,2:T(8,128)(2,1)}), bf16[1,128,4,512]{1,3,0,2:T(8,128)(2,1)S(1)}, u32[]{:S(2)}, u32[]{:S(2)}) %all-to-all-start) | async-done | bytes 524320 | tf_op jit(solution)/shard_map/all_to_all | solution.py:105
  29.5 3.6 %all-to-all-start.1 = ((bf16[1,128,4,512]{1,3,0,2:T(8,128)(2,1)}), bf16[1,128,4,512]{1,3,0,2:T(8,128)(2,1)S(1)}, u32[]{:S(2)}, u32[]{:S(2)}) async-start(bf16[1,128,4,512]{1,3,0,2:T(8,128)(2,1)} %bitcast.10), calls=%async_computation.1 | async-start | bytes 1048576 | tf_op jit(solution)/shard_map/all_to_all | solution.py:104
  33.4 1.1 copy.26
  34.4 12.7 %all-to-all-done.1 = bf16[1,128,4,512]{1,3,0,2:T(8,128)(2,1)S(1)} async-done(((bf16[1,128,4,512]{1,3,0,2:T(8,128)(2,1)}), bf16[1,128,4,512]{1,3,0,2:T(8,128)(2,1)S(1)}, u32[]{:S(2)}, u32[]{:S(2)}) %all-to-all-start.1) | async-done | bytes 524320 | tf_op jit(solution)/shard_map/all_to_all | solution.py:104
  47.1 4.2 %all-to-all-start.2 = ((bf16[1,128,4,512]{3,1,0,2:T(8,128)(2,1)}), bf16[1,128,4,512]{3,1,0,2:T(8,128)(2,1)}, u32[]{:S(2)}, u32[]{:S(2)}) async-start(bf16[1,128,4,512]{3,1,0,2:T(8,128)(2,1)} %copy.26), calls=%async_computation.2 | async-start | bytes 1048576 | tf_op jit(solution)/shard_map/all_to_all | solution.py:106
  51.8 0.7 copy.22
  53.0 0.7 copy.24
  54.1 11.3 %all-to-all-done.2 = bf16[1,128,4,512]{3,1,0,2:T(8,128)(2,1)} async-done(((bf16[1,128,4,512]{3,1,0,2:T(8,128)(2,1)}), bf16[1,128,4,512]{3,1,0,2:T(8,128)(2,1)}, u32[]{:S(2)}, u32[]{:S(2)}) %all-to-all-start.2) | async-done | bytes 524320 | tf_op jit(solution)/shard_map/all_to_all | solution.py:106
  65.4 1.2 reshape.146
  67.9 1.1 pad_maximum_fusion
  69.0 26.1 %while.54 = (s32[]{:T(128)}, bf16[4,512,128]{1,2,0:T(8,128)(2,1)S(1)}, s32[4]{0:T(128)S(1)}, bf16[512,4,2,64]{0,3,2,1:T(8,128)(2,1)}, bf16[512,4,2,64]{0,3,2,1:T...) while((s32[]{:T(128)}, ...), condition=%wide.region_8.9_spmd, body=%wide.region_2.8_spmd.sunk | while | flops 138281984 | bytes 9979571 | solution.py:128
  69.1 0.6 dynamic_slice.79
  71.7 2.0 %fusion.54 = (f32[2,512]{1,0:T(2,128)S(1)}, f32[2,512,512]{1,2,0:T(8,128)S(1)}) fusion(pred[512,512]{0,1:T(8,128)(4,1)S(1)} %iota_compare_fusion.2, bf16[512,4,2,64]{0,3,2,1:T(8,128)(2,1)} %get-tuple-element.423, s32[]{:T(128)S(6)} %select_n.36, bf16[512,4,2,64]{0,3,2,1:T(8,128)(2,1)} %get-tuple-element.424), kind=kOutput, calls=%fused_computation.62.clone.1 | convolution fusion | flops 69206528 | bytes 2626560 | tf_op jit(solution)/shard_map/while/body/eval_jaxpr/while/body/eval_jaxpr/sub | solution.py:75
  73.9 0.6 dynamic_slice.80
  74.5 0.9 multiply_reduce_fusion.4
  75.6 0.6 dynamic_slice.79
  78.2 2.0 %fusion.54 = (f32[2,512]{1,0:T(2,128)S(1)}, f32[2,512,512]{1,2,0:T(8,128)S(1)}) fusion(pred[512,512]{0,1:T(8,128)(4,1)S(1)} %iota_compare_fusion.2, bf16[512,4,2,64]{0,3,2,1:T(8,128)(2,1)} %get-tuple-element.423, s32[]{:T(128)S(6)} %select_n.36, bf16[512,4,2,64]{0,3,2,1:T(8,128)(2,1)} %get-tuple-element.424), kind=kOutput, calls=%fused_computation.62.clone.1 | convolution fusion | flops 69206528 | bytes 2626560 | tf_op jit(solution)/shard_map/while/body/eval_jaxpr/while/body/eval_jaxpr/sub | solution.py:75
  80.4 0.6 dynamic_slice.80
  81.0 0.9 multiply_reduce_fusion.4
  82.1 0.6 dynamic_slice.79
  84.7 2.0 %fusion.54 = (f32[2,512]{1,0:T(2,128)S(1)}, f32[2,512,512]{1,2,0:T(8,128)S(1)}) fusion(pred[512,512]{0,1:T(8,128)(4,1)S(1)} %iota_compare_fusion.2, bf16[512,4,2,64]{0,3,2,1:T(8,128)(2,1)} %get-tuple-element.423, s32[]{:T(128)S(6)} %select_n.36, bf16[512,4,2,64]{0,3,2,1:T(8,128)(2,1)} %get-tuple-element.424), kind=kOutput, calls=%fused_computation.62.clone.1 | convolution fusion | flops 69206528 | bytes 2626560 | tf_op jit(solution)/shard_map/while/body/eval_jaxpr/while/body/eval_jaxpr/sub | solution.py:75
  86.9 0.6 dynamic_slice.80
  87.5 0.9 multiply_reduce_fusion.4
  91.2 2.0 %fusion.54 = (f32[2,512]{1,0:T(2,128)S(1)}, f32[2,512,512]{1,2,0:T(8,128)S(1)}) fusion(pred[512,512]{0,1:T(8,128)(4,1)S(1)} %iota_compare_fusion.2, bf16[512,4,2,64]{0,3,2,1:T(8,128)(2,1)} %get-tuple-element.423, s32[]{:T(128)S(6)} %select_n.36, bf16[512,4,2,64]{0,3,2,1:T(8,128)(2,1)} %get-tuple-element.424), kind=kOutput, calls=%fused_computation.62.clone.1 | convolution fusion | flops 69206528 | bytes 2626560 | tf_op jit(solution)/shard_map/while/body/eval_jaxpr/while/body/eval_jaxpr/sub | solution.py:75
  93.5 0.6 dynamic_slice.80
  94.0 0.9 multiply_reduce_fusion.4
  95.3 16.4 %all_to_all.38 = bf16[4,1,128,1,512]{2,4,3,1,0:T(8,128)(2,1)S(1)} all-to-all(bf16[4,1,128,1,512]{2,4,3,1,0:T(8,128)(2,1)S(1)} %pad_maximum_fusion.2), channel_id=1, replica_groups=mesh['grp'=2,'sp'=4,'dp'=4] {'sp'}, dimensions={0} | all-to-all | bytes 1048576 | tf_op jit(solution)/shard_map/all_to_all | solution.py:9
  111.7 5.5 %fusion.38 = bf16[1,128,2048]{2,1,0:T(8,128)(2,1)} fusion(bf16[128,2048]{0,1:T(8,128)(2,1)S(1)} %bitcast.90, bf16[2048,2048]{1,0:T(8,128)(2,1)} %all-gather.2.cloned.1.call-done), kind=kOutput, calls=%fused_computation.38 | convolution fusion | flops 1074003968 | bytes 9437184 | tf_op jit(solution)/shard_map/dot_general | solution.py:132
  (55 shorter events, 5.8 us)
Async XLA Ops:
  6.5 1.0 copy-start
  6.5 8.4 %copy-start.1 = (bf16[1,128,2048]{2,1,0:T(8,128)(2,1)S(1)}, bf16[1,128,2048]{2,1,0:T(8,128)(2,1)}, u32[]{:S(2)}) copy-start(bf16[1,128,2048]{2,1,0:T(8,128)(2,1)} %param.12) | copy-start | bytes 1572868
  6.5 105.2 %all-gather.2.cloned.1.call-start = ((), (), s32[]{:S(2)}) async-start(), calls=%async_computation.4 | async-start | bytes 10485760 | tf_op jit(solution)/shard_map/all_gather | solution.py:134
  7.6 25.5 %copy-start.2 = (bf16[1,128,2048]{2,1,0:T(8,128)(2,1)S(1)}, bf16[1,128,2048]{2,1,0:T(8,128)(2,1)}, u32[]{:S(2)}) copy-start(bf16[1,128,2048]{2,1,0:T(8,128)(2,1)} %param.14) | copy-start | bytes 1572868
  8.6 20.8 %all-to-all-start = ((bf16[1,128,4,512]{1,3,0,2:T(8,128)(2,1)}), bf16[1,128,4,512]{1,3,0,2:T(8,128)(2,1)S(1)}, u32[]{:S(2)}, u32[]{:S(2)}) async-start(bf16[1,128,4,512]{1,3,0,2:T(8,128)(2,1)} %bitcast.7), calls=%async_computation | async-start | bytes 1048576 | tf_op jit(solution)/shard_map/all_to_all | solution.py:105
  29.5 21.8 %copy-start.7 = (f32[16]{0:T(128)S(1)}, f32[16]{0:T(128)}, u32[]{:S(2)}) copy-start(f32[16]{0:T(128)} %param.17) | copy-start | bytes 196
  29.5 17.6 %all-to-all-start.1 = ((bf16[1,128,4,512]{1,3,0,2:T(8,128)(2,1)}), bf16[1,128,4,512]{1,3,0,2:T(8,128)(2,1)S(1)}, u32[]{:S(2)}, u32[]{:S(2)}) async-start(bf16[1,128,4,512]{1,3,0,2:T(8,128)(2,1)} %bitcast.10), calls=%async_computation.1 | async-start | bytes 1048576 | tf_op jit(solution)/shard_map/all_to_all | solution.py:104
  47.1 18.3 %all-to-all-start.2 = ((bf16[1,128,4,512]{3,1,0,2:T(8,128)(2,1)}), bf16[1,128,4,512]{3,1,0,2:T(8,128)(2,1)}, u32[]{:S(2)}, u32[]{:S(2)}) async-start(bf16[1,128,4,512]{3,1,0,2:T(8,128)(2,1)} %copy.26), calls=%async_computation.2 | async-start | bytes 1048576 | tf_op jit(solution)/shard_map/all_to_all | solution.py:106
  65.4 1.6 %copy-start.5 = (f32[64]{0:T(128)S(1)}, f32[64]{0:T(128)}, u32[]{:S(2)}) copy-start(f32[64]{0:T(128)} %param.16) | copy-start | bytes 772
  66.6 0.7 copy-start.6
  67.6 1.5 %copy-start.3 = (bf16[4,512,128]{1,2,0:T(8,128)(2,1)S(1)}, bf16[4,512,128]{1,2,0:T(8,128)(2,1)}, u32[]{:S(2)}) copy-start(bf16[4,512,128]{1,2,0:T(8,128)(2,1)} %custom-call) | copy-start | bytes 1572868
  67.6 1.5 %copy-start.4 = (f32[128]{0:T(128)S(1)}, f32[128]{0:T(128)}, u32[]{:S(2)}) copy-start(f32[128]{0:T(128)} %param.18) | copy-start | bytes 1540
Sparse Core Ops, SparseCore 0:
  8.9 60.9 all-gather.1
